TPU v7x, 32 devices: a whole 2x2x4 slice. The times are simulated.
32 devices in a mesh: sp: 4 (over y, x), tp: 8 (over z, core).
Axes of the slice: x: 2, y: 2, z: 4, core: 2. Of those that a mesh axis runs over, the one named last changes fastest.
Arguments:
- queries: bfloat16 [4096, 2048], P('sp', 'tp'), may hold values from -160 to 160
- key_heads: bfloat16 [4096, 512], P('sp'), may hold values from -8 to 8
- value_heads: bfloat16 [4096, 512], P('sp'), may hold values from -4 to 4
- sink_logit: float32 [16], P('tp'), may hold values from -2 to 7
- out_weight: bfloat16 [2048, 2048], P('tp'), may hold values from -0.125 to 0.125
- residual: bfloat16 [4096, 2048], P(('sp', 'tp')), may hold values from -6 to 6
- mixer_gain: float32 [2048], replicated, may hold values from 0.1 to 1.9
- expert_gain: float32 [2048], replicated, may hold values from 0.1 to 1.9
- route_group: int32 [4096], P(('sp', 'tp')), may hold values from 0 to 3, as said below
- route_member: int32 [4096, 2], P(('sp', 'tp')), may hold values from 0 to 2, as said below
- route_weight: bfloat16 [4096, 2], P(('sp', 'tp')), may hold values from 0.19921875 to 1
- gate_weight: bfloat16 [12, 2048, 2048], P('sp', None, 'tp'), may hold values from -0.125 to 0.125
- up_weight: bfloat16 [12, 2048, 2048], P('sp', None, 'tp'), may hold values from -0.125 to 0.125
- down_weight: bfloat16 [12, 2048, 2048], P('sp', 'tp'), may hold values from -0.125 to 0.125
Outputs:
- output: bfloat16 [4096, 2048], P(('sp', 'tp'))
Inputs may be any that keep to these rules, and one draw needn't show every extreme that they name: `route_group`: among the tokens of one device, at most 40 name one group; in every draw one group is named by exactly 40 tokens of every device. `route_member`: the two entries of a token are different members of its group.
All inputs are finite; a program needn't handle non-finite values.
Results may differ from a plain program's by a relative error of at most 0.018.
Values may be sent and summed in bfloat16 or wider, within the bound.
A program may use at most 128 MiB of HBM per device.

v0:
```python
import jax
import jax.numpy as jnp
from jax import lax
from jax.sharding import PartitionSpec as P

HEADS = 16
KV_HEADS = 4
HEAD_DIM = 128
WINDOW = 128
BLOCK = 128
GROUP_EXPERTS = 3
EPS = 1e-06
NEG_BIG = -1e30


def extended(block, sides, width):
    for axis, dim in sides:
        count = lax.axis_size(axis)
        forward = [(i, i + 1) for i in range(count - 1)]
        backward = [(target, source) for source, target in forward]
        low = lax.ppermute(
            lax.slice_in_dim(block, block.shape[dim] - width, None, axis=dim), axis, forward
        )
        high = lax.ppermute(lax.slice_in_dim(block, 0, width, axis=dim), axis, backward)
        block = jnp.concatenate([low, block, high], axis=dim)
    return block


def window_attention(queries, key_heads, value_heads, sink_logit):
    seq_rows = queries.shape[0]
    heads_dev = sink_logit.shape[0]
    key_group = HEADS // KV_HEADS
    key_start = lax.axis_index("tp") * heads_dev // key_group * HEAD_DIM
    key_own = lax.dynamic_slice_in_dim(key_heads, key_start, HEAD_DIM, 1)
    value_own = lax.dynamic_slice_in_dim(value_heads, key_start, HEAD_DIM, 1)
    padded = extended(jnp.stack([key_own, value_own]), (("sp", 1),), WINDOW)
    blocks = seq_rows // BLOCK
    extent = WINDOW // BLOCK
    tile_rows = padded.reshape(2, blocks + 2 * extent, BLOCK, HEAD_DIM)
    key_spans = jnp.concatenate(
        [tile_rows[:, shifted : shifted + blocks] for shifted in range(2 * extent + 1)], axis=2
    )
    offset = lax.axis_index("sp") * seq_rows
    seq_total = seq_rows * lax.axis_size("sp")
    query_pos = offset + jnp.arange(seq_rows, dtype=jnp.int32).reshape(blocks, BLOCK)
    key_pos = (
        offset
        + (jnp.arange(blocks, dtype=jnp.int32) * BLOCK)[:, None]
        + jnp.arange(BLOCK + 2 * WINDOW, dtype=jnp.int32)[None, :]
        - WINDOW
    )
    inside = (
        (jnp.abs(query_pos[:, :, None] - key_pos[:, None, :]) <= WINDOW)
        & (key_pos >= 0)[:, None, :]
        & (key_pos < seq_total)[:, None, :]
    )
    query_blocks = queries.reshape(blocks, BLOCK, heads_dev, HEAD_DIM)
    scores = jnp.einsum(
        "nqhd,nkd->nhqk", query_blocks, key_spans[0], preferred_element_type=jnp.float32
    ) * HEAD_DIM ** (-0.5)
    scores = jnp.where(inside[:, None], scores, NEG_BIG)
    sink_col = sink_logit[None, :, None, None]
    row_top = jnp.maximum(jnp.max(scores, axis=3, keepdims=True), sink_col)
    exp_terms = jnp.exp(scores - row_top)
    row_mass = jnp.sum(exp_terms, axis=3, keepdims=True) + jnp.exp(sink_col - row_top)
    weight = (exp_terms / row_mass).astype(jnp.bfloat16)
    attended = jnp.einsum(
        "nhqk,nkd->nqhd", weight, key_spans[1], preferred_element_type=jnp.float32
    ).astype(jnp.bfloat16)
    return attended.reshape(seq_rows, heads_dev * HEAD_DIM)


def per_device(
    queries,
    key_heads,
    value_heads,
    sink_logit,
    out_weight,
    residual,
    mixer_gain,
    expert_gain,
    route_group,
    route_member,
    route_weight,
    gate_weight,
    up_weight,
    down_weight,
):
    attended = window_attention(queries, key_heads, value_heads, sink_logit)
    tok_rows = residual.shape[0]
    width = out_weight.shape[1]
    projected = lax.psum_scatter(
        jnp.dot(attended, out_weight, preferred_element_type=jnp.float32).astype(jnp.bfloat16),
        "tp",
        scatter_dimension=0,
        tiled=True,
    ).astype(jnp.float32)
    proj_scale = lax.rsqrt(jnp.mean(projected * projected, axis=1, keepdims=True) + EPS)
    mixed_rows = (residual.astype(jnp.float32) + mixer_gain * (projected * proj_scale)).astype(
        jnp.bfloat16
    )
    mixed_float = mixed_rows.astype(jnp.float32)
    norm_scale = lax.rsqrt(jnp.mean(mixed_float * mixed_float, axis=1, keepdims=True) + EPS)
    normed = (mixed_float * norm_scale * expert_gain).astype(jnp.bfloat16)
    groups = lax.axis_size("sp")
    capacity = max(2, (5 * tok_rows + 4 * groups - 1) // (4 * groups))
    group_ids = jnp.arange(groups, dtype=jnp.int32)
    chosen = (route_group[:, None] == group_ids[None, :]).astype(jnp.int32)
    group_rank = jnp.sum(chosen * (jnp.cumsum(chosen, axis=0) - 1), axis=1)
    slot_ids = route_group * capacity + group_rank
    placing = (jnp.arange(groups * capacity, dtype=jnp.int32)[:, None] == slot_ids[None, :]).astype(
        jnp.bfloat16
    )
    member_ids = jnp.arange(GROUP_EXPERTS, dtype=jnp.int32)
    token_gates = jnp.sum(
        route_weight.astype(jnp.float32)[:, :, None]
        * (route_member[:, :, None] == member_ids[None, None, :]).astype(jnp.float32),
        axis=1,
    ).astype(jnp.bfloat16)
    send_rows = (
        jnp.dot(placing, normed, preferred_element_type=jnp.float32)
        .astype(jnp.bfloat16)
        .reshape(groups, capacity, width)
    )
    send_gates = (
        jnp.dot(placing, token_gates, preferred_element_type=jnp.float32)
        .astype(jnp.bfloat16)
        .reshape(groups, capacity, GROUP_EXPERTS)
    )
    arrived_rows, arrived_gates = (
        lax.all_to_all(send_rows, "sp", split_axis=0, concat_axis=0, tiled=True),
        lax.all_to_all(send_gates, "sp", split_axis=0, concat_axis=0, tiled=True),
    )
    pooled_rows, pooled_gates = (
        lax.all_gather(arrived_rows, "tp", axis=0, tiled=True),
        lax.all_gather(arrived_gates, "tp", axis=0, tiled=True),
    )
    flat_rows = pooled_rows.reshape(-1, width)
    flat_gates = pooled_gates.reshape(-1, GROUP_EXPERTS).astype(jnp.float32)
    gate_pre = jnp.einsum("md,edh->meh", flat_rows, gate_weight, preferred_element_type=jnp.float32)
    up_pre = jnp.einsum("md,edh->meh", flat_rows, up_weight, preferred_element_type=jnp.float32)
    hidden = (jax.nn.silu(gate_pre) * up_pre * flat_gates[:, :, None]).astype(jnp.bfloat16)
    partial_out = jnp.einsum("meh,ehd->md", hidden, down_weight, preferred_element_type=jnp.float32)
    summed = lax.psum_scatter(
        partial_out.reshape(pooled_rows.shape).astype(jnp.bfloat16),
        "tp",
        scatter_dimension=0,
        tiled=True,
    )
    returned = lax.all_to_all(summed, "sp", split_axis=0, concat_axis=0, tiled=True)
    expert_out = lax.dot_general(
        placing,
        returned.reshape(groups * capacity, width),
        (((0,), (0,)), ((), ())),
        preferred_element_type=jnp.float32,
    )
    return (mixed_float + expert_out).astype(jnp.bfloat16)


def solution(mesh):
    placed = (
        P("sp", "tp"),
        P("sp", None),
        P("sp", None),
        P("tp"),
        P("tp", None),
        P(("sp", "tp"), None),
        P(),
        P(),
        P(("sp", "tp")),
        P(("sp", "tp"), None),
        P(("sp", "tp"), None),
        P("sp", None, "tp"),
        P("sp", None, "tp"),
        P("sp", "tp", None),
    )
    return jax.shard_map(
        per_device, mesh=mesh, in_specs=placed, out_specs=P(("sp", "tp"), None), check_vma=False
    )
```

profile of v0, /device:TPU:0, one launch (start us, length us, event | category | flops | bytes accessed | tf_op | source)
XLA Modules:
  0.0 256.5 jit_solution(17460790023405655798)
XLA Ops:
  6.5 1.2 dynamic-slice_bitcast_fusion
  7.8 0.7 copy-done.2
  8.5 0.6 pad_maximum_fusion.3
  9.1 4.9 %collective-permute-start = (bf16[2,128,128]{2,1,0:T(8,128)(2,1)}, bf16[2,128,128]{2,1,0:T(8,128)(2,1)S(1)}, u32[]{:S(2)}, u32[]{:S(2)}) collective-permute-start(bf16[2,128,128]{2,1,0:T(8,128)(2,1)} %get-tuple-element.10), channel_id=1, source_target_pairs={{0,8},{8,16},{16,24},{1,9},{9,17},{17,25},{2,10},{10,18},{18,26},{... | collective-permute-start | bytes 196616 | tf_op jit(solution)/shard_map/ppermute | solution.py:21
  14.0 1.3 collective-permute-start.1
  15.3 0.1 fusion.29
  15.4 0.1 add_add_fusion
  15.5 3.0 %fusion.6 = pred[8,128,384]{1,2,0:T(8,128)(4,1)} fusion(s32[8,384]{1,0:T(8,128)S(1)} %add_add_fusion, s32[8,128]{1,0:T(8,128)S(1)} %add_add_fusion.1, pred[8,384]{1,0:T(8,128)(4,1)S(1)} %get-tuple-element.13, pred[8,384]{1,0:T(8,128)(4,1)S(1)} %get-tuple-element.12), kind=kLoop, calls=%fused_computation.18 | loop fusion | flops 1966080 | bytes 415744 | tf_op jit(solution)/shard_map/and | solution.py:53
  18.5 2.0 reshape.151
  20.4 1.0 pad_maximum_fusion.1
  21.5 0.4 fusion.36
  21.9 0.1 pad_maximum_fusion
  22.0 0.5 copy-done.3
  22.5 0.2 copy-done.5
  22.7 0.6 fusion.4
  23.3 0.0 copy-done.9
  23.3 0.1 broadcast_maximum_fusion
  23.4 0.7 fusion.2
  24.1 0.1 exponential_add_fusion
  24.2 1.1 fusion.9
  25.3 0.3 copy.50
  25.7 3.2 %convolution_convert_fusion = bf16[1024,2048]{1,0:T(8,128)(2,1)} fusion(bf16[256,2048]{1,0:T(8,128)(2,1)S(1)} %copy-done.4, bf16[32,8,8,128]{3,2,1,0:T(8,128)(2,1)S(1)} %bitcast.64), kind=kOutput, calls=%fused_computation.3 | convolution fusion | flops 1075838976 | bytes 5767168 | tf_op jit(solution)/shard_map/dot_general | solution.py:93
  28.9 0.0 reduce-scatter.3.cloned.1.call-update
  28.9 0.0 all-gather.2.cloned.1.call-start
  29.0 0.6 copy-done.8
  29.5 0.1 fusion.24
  29.6 0.2 reduce_window_sum.11
  29.8 0.2 select_reduce_fusion
  30.0 52.0 %reduce-scatter.3.cloned.1.call-done = bf16[128,2048]{1,0:T(8,128)(2,1)} async-done(((bf16[1024,2048]{1,0:T(8,128)(2,1)}), bf16[128,2048]{1,0:T(8,128)(2,1)}) %reduce-scatter.3.cloned.1.call-update) | async-done | bytes 524304 | tf_op jit(solution)/shard_map/reduce_scatter | solution.py:92
  82.0 1.2 fusion.10
  83.2 1.6 fusion.14
  84.8 0.8 copy-done.1
  85.6 0.4 convolution_convert_fusion.1
  86.0 11.6 %all_to_all.15 = bf16[4,40,2048]{2,1,0:T(8,128)(2,1)} all-to-all(bf16[4,40,2048]{2,1,0:T(8,128)(2,1)S(1)} %bitcast.66), channel_id=1, replica_groups=mesh['sp'=4,'tp'=8] {'sp'}, dimensions={0} | all-to-all | bytes 1310720 | tf_op jit(solution)/shard_map/all_to_all | solution.py:131
  97.7 0.0 all-gather.2.cloned.1.call-update
  97.7 0.0 reduce-scatter.5.cloned.1.call-start
  97.8 0.1 convolution_convert_fusion.2
  97.9 0.1 reshape.155
  98.0 7.0 %all_to_all.16 = bf16[4,40,3]{1,2,0:T(4,128)(2,1)S(1)} all-to-all(bf16[4,40,3]{1,2,0:T(4,128)(2,1)S(1)} %copy.51), channel_id=1, replica_groups=mesh['sp'=4,'tp'=8] {'sp'}, dimensions={0} | all-to-all | bytes 1920 | tf_op jit(solution)/shard_map/all_to_all | solution.py:132
  105.1 15.2 %all_gather.7 = bf16[32,40,3]{1,2,0:T(4,128)(2,1)S(1)} all-gather(bf16[4,40,3]{1,2,0:T(4,128)(2,1)S(1)} %all_to_all.16), channel_id=1, replica_groups=mesh['sp'=4,'tp'=8] {'tp'}, dimensions={0}, use_global_device_ids=true | all-gather | bytes 8640 | tf_op jit(solution)/shard_map/all_gather | solution.py:136
  120.3 0.1 reshape.157
  120.4 32.6 %all-gather.2.cloned.1.call-done = bf16[32,40,2048]{2,1,0:T(8,128)(2,1)} async-done(((bf16[4,40,2048]{2,1,0:T(8,128)(2,1)}), bf16[32,40,2048]{2,1,0:T(8,128)(2,1)}) %all-gather.2.cloned.1.call-update) | async-done | bytes 5242896 | tf_op jit(solution)/shard_map/all_gather | solution.py:135
  152.9 9.7 %fusion.37 = f32[1280,3,256]{2,0,1:T(8,128)} fusion(bf16[1280,2048,1]{1,0,2:T(8,128)(2,1)} %bitcast.67, bf16[3,2048,256]{2,1,0:T(8,128)(2,1)} %param.25), kind=kOutput, calls=%fused_computation.70 | convolution fusion | flops 4026531840 | bytes 12320768 | tf_op jit(solution)/shard_map/md,edh->meh/dot_general | solution.py:140
  162.6 14.6 %bitcast_convert_fusion = bf16[1280,2048]{1,0:T(8,128)(2,1)} fusion(bf16[3,256,2048]{2,1,0:T(8,128)(2,1)S(1)} %copy-done, bf16[1280,2048,1]{1,0,2:T(8,128)(2,1)} %bitcast.68, bf16[3,2048,256]{2,1,0:T(8,128)(2,1)} %param.26, f32[1280,3,256]{2,0,1:T(8,128)} %fusion.37, f32[1280,3]{0,1:T(4,128)S(1)} %reshape.157), kind=kOutput, calls=%fused_computation | convolution fusion | flops 8062566400 | bytes 20724736 | tf_op jit(solution)/shard_map/meh,ehd->md/dot_general | solution.py:143
  177.2 0.0 reduce-scatter.5.cloned.1.call-update
  177.2 58.7 %reduce-scatter.5.cloned.1.call-done = bf16[4,40,2048]{2,1,0:T(8,128)(2,1)} async-done(((bf16[32,40,2048]{2,1,0:T(8,128)(2,1)}), bf16[4,40,2048]{2,1,0:T(8,128)(2,1)}) %reduce-scatter.5.cloned.1.call-update) | async-done | bytes 655376 | tf_op jit(solution)/shard_map/reduce_scatter | solution.py:144
  236.0 11.8 %all_to_all.17 = bf16[4,40,2048]{2,1,0:T(8,128)(2,1)S(1)} all-to-all(bf16[4,40,2048]{2,1,0:T(8,128)(2,1)} %reduce-scatter.5.cloned.1.call-done), channel_id=1, replica_groups=mesh['sp'=4,'tp'=8] {'sp'}, dimensions={0} | all-to-all | bytes 1310720 | tf_op jit(solution)/shard_map/all_to_all | solution.py:150
  247.7 2.2 fusion.3
  (30 shorter events, 0.1 us)
Async XLA Ops:
  6.5 156.1 %copy-start = (bf16[3,256,2048]{2,1,0:T(8,128)(2,1)S(1)}, bf16[3,256,2048]{2,1,0:T(8,128)(2,1)}, u32[]{:S(2)}) copy-start(bf16[3,256,2048]{2,1,0:T(8,128)(2,1)} %param.27) | copy-start | bytes 9437188
  6.5 75.4 %reduce-scatter.3.cloned.1.call-start = ((), (), s32[]{:S(2)}) async-start(), calls=%async_computation.5 | async-start | bytes 4718592 | tf_op jit(solution)/shard_map/reduce_scatter | solution.py:92
  7.8 0.7 copy-start.2
  9.1 11.3 %collective-permute-start = (bf16[2,128,128]{2,1,0:T(8,128)(2,1)}, bf16[2,128,128]{2,1,0:T(8,128)(2,1)S(1)}, u32[]{:S(2)}, u32[]{:S(2)}) collective-permute-start(bf16[2,128,128]{2,1,0:T(8,128)(2,1)} %get-tuple-element.10), channel_id=1, source_target_pairs={{0,8},{8,16},{16,24},{1,9},{9,17},{17,25},{2,10},{10,18},{18,26},{... | collective-permute-start | bytes 196616 | tf_op jit(solution)/shard_map/ppermute | solution.py:21
  14.0 6.5 %collective-permute-start.1 = (bf16[2,128,128]{2,1,0:T(8,128)(2,1)S(1)}, bf16[2,128,128]{2,1,0:T(8,128)(2,1)}, u32[]{:S(2)}, u32[]{:S(2)}) collective-permute-start(bf16[2,128,128]{2,1,0:T(8,128)(2,1)S(1)} %get-tuple-element.11), channel_id=1, source_target_pairs={{8,0},{16,8},{24,16},{9,1},{17,9},{25,17},{10,2},{18,10},{26,18},{... | collective-permute-start | bytes 196616 | tf_op jit(solution)/shard_map/ppermute | solution.py:24
  21.5 1.0 copy-start.3
  21.5 1.2 copy-start.5
  22.6 0.7 copy-start.9
  24.2 1.4 copy-start.4
  28.9 0.7 copy-start.8
  28.9 54.3 %copy-start.6 = (f32[2048]{0:T(1024)S(1)}, f32[2048]{0:T(1024)}, u32[]{:S(2)}) copy-start(f32[2048]{0:T(1024)} %param.20) | copy-start | bytes 24580
  28.9 56.7 %copy-start.7 = (f32[2048]{0:T(1024)S(1)}, f32[2048]{0:T(1024)}, u32[]{:S(2)}) copy-start(f32[2048]{0:T(1024)} %param.21) | copy-start | bytes 24580
  28.9 68.8 %copy-start.11 = (bf16[128,2]{0,1:T(2,128)(2,1)S(1)}, bf16[128,2]{0,1:T(2,128)(2,1)}, u32[]{:S(2)}) copy-start(bf16[128,2]{0,1:T(2,128)(2,1)} %param.24) | copy-start | bytes 1540
  28.9 68.8 %copy-start.10 = (s32[128,2]{0,1:T(2,128)S(1)}, s32[128,2]{0,1:T(2,128)}, u32[]{:S(2)}) copy-start(s32[128,2]{0,1:T(2,128)} %param.23) | copy-start | bytes 3076
  28.9 124.0 %all-gather.2.cloned.1.call-start = ((), (), s32[]{:S(2)}) async-start(), calls=%async_computation.6 | async-start | bytes 5898240 | tf_op jit(solution)/shard_map/all_gather | solution.py:135
  84.8 0.8 copy-start.1
  97.7 138.3 %reduce-scatter.5.cloned.1.call-start = ((), (), s32[]{:S(2)}) async-start(), calls=%async_computation.7 | async-start | bytes 5898240 | tf_op jit(solution)/shard_map/reduce_scatter | solution.py:144
Sparse Core Ops, SparseCore 0:
  29.0 52.8 reduce-scatter.2
  97.8 55.0 all-gather.1
  177.4 58.5 reduce-scatter.4
where the time goes:
time: 257 us; the launch traced here: 256 us
  waiting for transfers between devices  143 us (56%)
  blocking collectives  45.6 us (18%)
  matrix products  32 us (12%)
  between operations  13.3 us (5%)
  other arithmetic  9.2 us (4%)
  local copies, waits for them, and re-layouts  6.79 us (3%)
  starting transfers between devices  6.24 us (2%)
    reduce_scatter x1, waiting for transfers between devices, per_device(): lax.psum_scatter(partial_out.reshape(pooled_rows.shape).astype(jnp.bfloat...  58.7 us
    reduce_scatter x1, waiting for transfers between devices, per_device(): lax.psum_scatter(jnp.dot(attended, out_weight, preferred_element_type=jnp...  52 us
    all_gather x1, waiting for transfers between devices, per_device(): lax.all_gather(arrived_rows, 'tp', axis=0, tiled=True)  32.6 us
    all_gather x1, blocking collectives, per_device(): lax.all_gather(arrived_gates, 'tp', axis=0, tiled=True)  15.2 us
    dot_general x1, matrix products, per_device(): jnp.einsum('meh,ehd->md', hidden, down_weight, preferred_element_type=jnp...  14.6 us
    all_to_all x1, blocking collectives, per_device(): lax.all_to_all(summed, 'sp', split_axis=0, concat_axis=0, tiled=True)  11.8 us
    all_to_all x1, blocking collectives, per_device(): lax.all_to_all(send_rows, 'sp', split_axis=0, concat_axis=0, tiled=True)  11.6 us
    dot_general x1, matrix products, per_device(): jnp.einsum('md,edh->meh', flat_rows, gate_weight, preferred_element_type=...  9.71 us
  transfers between devices with their start and end apart: 5, of which 3 were waited for; matrix products, arithmetic and copies ran while one was open for 2% of the time, Pallas kernels for 0%

commit v1 on v0

--- a/solution.py
+++ b/solution.py
@@ -11,6 +11,13 @@
 GROUP_EXPERTS = 3
 EPS = 1e-06
 NEG_BIG = -1e30
+
+
+def swapped_in(x, axis, d):
+    devices = lax.axis_size(axis)
+    tiles = jnp.stack([x for _ in range(devices)])
+    tiles = lax.all_to_all(tiles, axis, split_axis=0, concat_axis=0)
+    return jnp.concatenate(tiles, axis=d)
 
 
 def extended(block, sides, width):
@@ -132,7 +139,7 @@
         lax.all_to_all(send_gates, "sp", split_axis=0, concat_axis=0, tiled=True),
     )
     pooled_rows, pooled_gates = (
-        lax.all_gather(arrived_rows, "tp", axis=0, tiled=True),
+        swapped_in(arrived_rows, "tp", 0),
         lax.all_gather(arrived_gates, "tp", axis=0, tiled=True),
     )
     flat_rows = pooled_rows.reshape(-1, width)

time: 257 us -> 333 us (1.30)
  blocking collectives: 45.6 us -> 146 us
  waiting for transfers between devices: 143 us -> 104 us
  starting transfers between devices: 6.24 us -> 16.3 us
  local copies, waits for them, and re-layouts: 6.79 us -> 10.4 us
    all_gather x1, blocking collectives: 15.2 us -> 122 us  [per_device(): lax.all_gather(arrived_gates, 'tp', axis=0, tiled=True)]
    all_gather x1 -> x0, waiting for transfers between devices: 32.6 us -> none  [per_device(): lax.all_gather(arrived_rows, 'tp', axis=0, tiled=True)]
    all_to_all x0 -> x2, starting transfers between devices: none -> 10.1 us  [the longest x1 5.46 us: per_device(): lax.all_to_all(send_gates, 'sp', split_axis=0, concat_axis=0, tiled=True)]
    all_to_all x1 -> x0, blocking collectives: 7.03 us -> none  [per_device(): lax.all_to_all(send_gates, 'sp', split_axis=0, concat_axis=0, tiled=True)]
    reduce_scatter x1, waiting for transfers between devices: 52 us -> 45.6 us  [per_device(): lax.psum_scatter(jnp.dot(attended, out_weight, preferred_element_type=jnp...]
  transfers between devices with their start and end apart: 5 -> 6, of which waited for: 3 -> 2; matrix products, arithmetic and copies ran while one was open for 2% -> 3% of each run, Pallas kernels for 0% -> 0%
where the time goes in v1:
time: 333 us
  blocking collectives  146 us (44%)
  waiting for transfers between devices  104 us (31%)
  matrix products  32.8 us (10%)
  starting transfers between devices  16.3 us (5%)
  between operations  13.6 us (4%)
  local copies, waits for them, and re-layouts  10.4 us (3%)
  other arithmetic  9.2 us (3%)
    all_gather x1, blocking collectives, per_device(): lax.all_gather(arrived_gates, 'tp', axis=0, tiled=True)  122 us
    reduce_scatter x1, waiting for transfers between devices, per_device(): lax.psum_scatter(partial_out.reshape(pooled_rows.shape).astype(jnp.bfloat...  58.7 us
    reduce_scatter x1, waiting for transfers between devices, per_device(): lax.psum_scatter(jnp.dot(attended, out_weight, preferred_element_type=jnp...  45.6 us
    dot_general x1, matrix products, per_device(): jnp.einsum('meh,ehd->md', hidden, down_weight, preferred_element_type=jnp...  14.6 us
    all_to_all x1, blocking collectives, per_device(): lax.all_to_all(summed, 'sp', split_axis=0, concat_axis=0, tiled=True)  11.8 us
    all_to_all x1, blocking collectives, per_device(): lax.all_to_all(send_rows, 'sp', split_axis=0, concat_axis=0, tiled=True)  11.8 us
    dot_general x1, matrix products, per_device(): jnp.einsum('md,edh->meh', flat_rows, gate_weight, preferred_element_type=...  9.71 us
  transfers between devices with their start and end apart: 6, of which 2 were waited for; matrix products, arithmetic and copies ran while one was open for 3% of the time, Pallas kernels for 0%

profile of v1, /device:TPU:0, one launch (start us, length us, event | category | flops | bytes accessed | tf_op | source)
XLA Modules:
  0.0 332.7 jit_solution(15827987099144155774)
XLA Ops:
  6.5 1.2 dynamic-slice_bitcast_fusion
  7.8 0.7 copy-done.2
  8.5 0.6 pad_maximum_fusion.3
  9.1 4.9 %collective-permute-start = (bf16[2,128,128]{2,1,0:T(8,128)(2,1)}, bf16[2,128,128]{2,1,0:T(8,128)(2,1)S(1)}, u32[]{:S(2)}, u32[]{:S(2)}) collective-permute-start(bf16[2,128,128]{2,1,0:T(8,128)(2,1)} %get-tuple-element.10), channel_id=1, source_target_pairs={{0,8},{8,16},{16,24},{1,9},{9,17},{17,25},{2,10},{10,18},{18,26},{... | collective-permute-start | bytes 196616 | tf_op jit(solution)/shard_map/ppermute | solution.py:28
  14.0 1.3 collective-permute-start.1
  15.3 0.1 fusion.29
  15.4 0.1 add_add_fusion
  15.4 3.0 fusion.6
  18.5 2.0 reshape.150
  20.4 1.0 pad_maximum_fusion.1
  21.5 0.4 fusion.36
  21.9 0.1 pad_maximum_fusion
  22.0 0.5 copy-done.3
  22.5 0.2 copy-done.5
  22.6 0.6 fusion.4
  23.3 0.0 copy-done.9
  23.3 0.1 broadcast_maximum_fusion
  23.4 0.7 fusion.2
  24.1 0.1 exponential_add_fusion
  24.2 1.1 fusion.9
  25.3 0.3 copy.50
  25.7 3.2 convolution_convert_fusion
  28.9 0.0 reduce-scatter.3.cloned.1.call-update
  28.9 0.6 copy-done.11
  29.6 0.1 fusion.24
  29.6 0.2 reduce_window_sum.11
  29.8 0.2 select_reduce_fusion
  30.0 0.1 convolution_convert_fusion.2
  30.2 0.1 reshape.153
  30.3 0.6 copy.51
  30.9 5.5 %all-to-all-start.2 = ((bf16[4,40,3]{1,2,0:T(4,128)(2,1)}), bf16[4,40,3]{1,2,0:T(4,128)(2,1)S(1)}, u32[]{:S(2)}, u32[]{:S(2)}) async-start(bf16[4,40,3]{1,2,0:T(4,128)(2,1)} %copy.51), calls=%async_computation.3 | async-start | bytes 8192 | tf_op jit(solution)/shard_map/all_to_all | solution.py:139
  36.3 45.6 %reduce-scatter.3.cloned.1.call-done = bf16[128,2048]{1,0:T(8,128)(2,1)} async-done(((bf16[1024,2048]{1,0:T(8,128)(2,1)}), bf16[128,2048]{1,0:T(8,128)(2,1)}) %reduce-scatter.3.cloned.1.call-update) | async-done | bytes 524304 | tf_op jit(solution)/shard_map/reduce_scatter | solution.py:99
  82.0 1.2 fusion.10
  83.2 1.6 fusion.14
  84.9 0.8 copy-done.1
  85.6 1.2 convolution_convert_fusion.1
  86.9 11.8 %all_to_all.20 = bf16[4,40,2048]{2,1,0:T(8,128)(2,1)S(1)} all-to-all(bf16[4,40,2048]{2,1,0:T(8,128)(2,1)} %bitcast.66), channel_id=1, replica_groups=mesh['sp'=4,'tp'=8] {'sp'}, dimensions={0} | all-to-all | bytes 1310720 | tf_op jit(solution)/shard_map/all_to_all | solution.py:138
  98.7 3.0 stack.11
  101.7 4.6 %all-to-all-start.1 = ((bf16[8,4,40,2048]{3,2,1,0:T(8,128)(2,1)}), bf16[8,4,40,2048]{3,2,1,0:T(8,128)(2,1)}, u32[]{:S(2)}, u32[]{:S(2)}) async-start(bf16[8,4,40,2048]{3,2,1,0:T(8,128)(2,1)} %stack.11), calls=%async_computation.2 | async-start | bytes 10485760 | tf_op jit(solution)/shard_map/all_to_all | solution.py:19
  106.3 0.0 reduce-scatter.5.cloned.1.call-start
  106.4 122.5 %all_gather.3 = bf16[32,40,3]{1,2,0:T(4,128)(2,1)S(1)} all-gather(bf16[4,40,3]{1,2,0:T(4,128)(2,1)S(1)} %all-to-all-done.2), channel_id=1, replica_groups=mesh['sp'=4,'tp'=8] {'tp'}, dimensions={0}, use_global_device_ids=true | all-gather | bytes 8640 | tf_op jit(solution)/shard_map/all_gather | solution.py:143
  228.8 0.1 reshape.155
  228.9 9.7 %fusion.37 = f32[1280,3,256]{2,0,1:T(8,128)} fusion(bf16[1280,2048,1]{1,0,2:T(8,128)(2,1)} %bitcast.12, bf16[3,2048,256]{2,1,0:T(8,128)(2,1)} %param.25), kind=kOutput, calls=%fused_computation.70 | convolution fusion | flops 4026531840 | bytes 12320768 | tf_op jit(solution)/shard_map/md,edh->meh/dot_general | solution.py:147
  238.7 14.6 %bitcast_convert_fusion = bf16[1280,2048]{1,0:T(8,128)(2,1)} fusion(bf16[3,256,2048]{2,1,0:T(8,128)(2,1)S(1)} %copy-done, bf16[1280,2048,1]{1,0,2:T(8,128)(2,1)} %bitcast.12, bf16[3,2048,256]{2,1,0:T(8,128)(2,1)} %param.26, f32[1280,3,256]{2,0,1:T(8,128)} %fusion.37, f32[1280,3]{0,1:T(4,128)S(1)} %reshape.155), kind=kOutput, calls=%fused_computation | convolution fusion | flops 8062566400 | bytes 20724736 | tf_op jit(solution)/shard_map/meh,ehd->md/dot_general | solution.py:150
  253.3 0.0 reduce-scatter.5.cloned.1.call-update
  253.3 58.7 %reduce-scatter.5.cloned.1.call-done = bf16[4,40,2048]{2,1,0:T(8,128)(2,1)} async-done(((bf16[32,40,2048]{2,1,0:T(8,128)(2,1)}), bf16[4,40,2048]{2,1,0:T(8,128)(2,1)}) %reduce-scatter.5.cloned.1.call-update) | async-done | bytes 655376 | tf_op jit(solution)/shard_map/reduce_scatter | solution.py:151
  311.9 11.8 %all_to_all.21 = bf16[4,40,2048]{2,1,0:T(8,128)(2,1)S(1)} all-to-all(bf16[4,40,2048]{2,1,0:T(8,128)(2,1)} %reduce-scatter.5.cloned.1.call-done), channel_id=1, replica_groups=mesh['sp'=4,'tp'=8] {'sp'}, dimensions={0} | all-to-all | bytes 1310720 | tf_op jit(solution)/shard_map/all_to_all | solution.py:157
  323.7 2.2 fusion.3
  (31 shorter events, 0.1 us)
Async XLA Ops:
  6.5 232.1 %copy-start = (bf16[3,256,2048]{2,1,0:T(8,128)(2,1)S(1)}, bf16[3,256,2048]{2,1,0:T(8,128)(2,1)}, u32[]{:S(2)}) copy-start(bf16[3,256,2048]{2,1,0:T(8,128)(2,1)} %param.27) | copy-start | bytes 9437188
  6.5 75.5 %reduce-scatter.3.cloned.1.call-start = ((), (), s32[]{:S(2)}) async-start(), calls=%async_computation.6 | async-start | bytes 4718592 | tf_op jit(solution)/shard_map/reduce_scatter | solution.py:99
  7.8 0.7 copy-start.2
  9.1 11.3 %collective-permute-start = (bf16[2,128,128]{2,1,0:T(8,128)(2,1)}, bf16[2,128,128]{2,1,0:T(8,128)(2,1)S(1)}, u32[]{:S(2)}, u32[]{:S(2)}) collective-permute-start(bf16[2,128,128]{2,1,0:T(8,128)(2,1)} %get-tuple-element.10), channel_id=1, source_target_pairs={{0,8},{8,16},{16,24},{1,9},{9,17},{17,25},{2,10},{10,18},{18,26},{... | collective-permute-start | bytes 196616 | tf_op jit(solution)/shard_map/ppermute | solution.py:28
  14.0 6.5 %collective-permute-start.1 = (bf16[2,128,128]{2,1,0:T(8,128)(2,1)S(1)}, bf16[2,128,128]{2,1,0:T(8,128)(2,1)}, u32[]{:S(2)}, u32[]{:S(2)}) collective-permute-start(bf16[2,128,128]{2,1,0:T(8,128)(2,1)S(1)} %get-tuple-element.11), channel_id=1, source_target_pairs={{8,0},{16,8},{24,16},{9,1},{17,9},{25,17},{10,2},{18,10},{26,18},{... | collective-permute-start | bytes 196616 | tf_op jit(solution)/shard_map/ppermute | solution.py:31
  21.5 1.0 copy-start.3
  21.5 1.2 copy-start.5
  22.6 0.7 copy-start.9
  24.2 1.4 copy-start.4
  28.9 0.7 copy-start.11
  28.9 0.7 copy-start.8
  28.9 0.9 copy-start.10
  28.9 54.3 %copy-start.6 = (f32[2048]{0:T(1024)S(1)}, f32[2048]{0:T(1024)}, u32[]{:S(2)}) copy-start(f32[2048]{0:T(1024)} %param.20) | copy-start | bytes 24580
  28.9 56.7 %copy-start.7 = (f32[2048]{0:T(1024)S(1)}, f32[2048]{0:T(1024)}, u32[]{:S(2)}) copy-start(f32[2048]{0:T(1024)} %param.21) | copy-start | bytes 24580
  30.9 56.0 %all-to-all-start.2 = ((bf16[4,40,3]{1,2,0:T(4,128)(2,1)}), bf16[4,40,3]{1,2,0:T(4,128)(2,1)S(1)}, u32[]{:S(2)}, u32[]{:S(2)}) async-start(bf16[4,40,3]{1,2,0:T(4,128)(2,1)} %copy.51), calls=%async_computation.3 | async-start | bytes 8192 | tf_op jit(solution)/shard_map/all_to_all | solution.py:139
  84.8 0.8 copy-start.1
  101.7 127.3 %all-to-all-start.1 = ((bf16[8,4,40,2048]{3,2,1,0:T(8,128)(2,1)}), bf16[8,4,40,2048]{3,2,1,0:T(8,128)(2,1)}, u32[]{:S(2)}, u32[]{:S(2)}) async-start(bf16[8,4,40,2048]{3,2,1,0:T(8,128)(2,1)} %stack.11), calls=%async_computation.2 | async-start | bytes 10485760 | tf_op jit(solution)/shard_map/all_to_all | solution.py:19
  106.3 205.6 %reduce-scatter.5.cloned.1.call-start = ((), (), s32[]{:S(2)}) async-start(), calls=%async_computation.7 | async-start | bytes 5898240 | tf_op jit(solution)/shard_map/reduce_scatter | solution.py:151
Sparse Core Ops, SparseCore 0:
  29.1 52.8 reduce-scatter.2
  253.4 58.4 reduce-scatter.4
